TPU v7x, 256 devices: a whole 4x4x8 slice. The times are simulated.
256 devices in a mesh: sp: 16 (over y, x), tp: 16 (over z, core).
Axes of the slice: x: 4, y: 4, z: 8, core: 2. Of those that a mesh axis runs over, the one named last changes fastest.
Arguments:
- query_a: bfloat16 [4096, 16, 256], P('sp', 'tp'), may hold values from -5.5 to 5.5
- key_a: bfloat16 [4096, 16, 256], P('sp', 'tp'), may hold values from -5.5 to 5.5
- value_a: bfloat16 [4096, 16, 256], P('sp', 'tp'), may hold values from -6 to 6
- query_b: bfloat16 [4096, 16, 128], P('sp', 'tp'), may hold values from -5.5 to 5.5
- key_b: bfloat16 [4096, 16, 128], P('sp', 'tp'), may hold values from -5.5 to 5.5
- value_b: bfloat16 [4096, 16, 128], P('sp', 'tp'), may hold values from -6 to 6
- lambdas: float32 [2, 16], P(None, 'tp'), may hold values from 0.3 to 0.8
- gain_a: float32 [256], replicated, may hold values from 0.1 to 1.9
- gain_b: float32 [128], replicated, may hold values from 0.1 to 1.9
- out_a: bfloat16 [4096, 4096], P('tp'), may hold values from -0.078125 to 0.078125
- out_b: bfloat16 [2048, 4096], P('tp'), may hold values from -0.078125 to 0.078125
- residual: bfloat16 [4096, 4096], P(('sp', 'tp')), may hold values from -6 to 6
- norm_gain: float32 [4096], replicated, may hold values from 0.1 to 1.9
- route_ids: int32 [4096, 2], P(('sp', 'tp')), may hold values from 0 to 31, all different within a row; in each aligned block of 16 rows (0 to 15, 16 to 31, ...) at most 2 rows name the same one
- route_weights: float32 [4096, 2], P(('sp', 'tp')), may hold values from 0.1 to 0.9
- w_gate: bfloat16 [32, 4096, 2048], P('sp', None, 'tp'), may hold values from -0.28125 to 0.28125
- w_up: bfloat16 [32, 4096, 2048], P('sp', None, 'tp'), may hold values from -0.28125 to 0.28125
- w_down: bfloat16 [32, 2048, 4096], P('sp', 'tp'), may hold values from -0.01977539 to 0.01977539
Outputs:
- result: bfloat16 [4096, 4096], P(('sp', 'tp'))
Inputs may be any that keep to these rules, and one draw needn't show every extreme that they name: `route_ids`: in the rows of one device each token names 2 different experts, no expert is named more than 2 times, a bound that some block reaches.
All inputs are finite; a program needn't handle non-finite values.
Results may differ from a plain program's by a relative error of at most 0.02.
Values may be sent and summed in bfloat16 or wider, within the bound.
No kernel may reach another device: no remote copies, remote signals or barrier semaphores. Data moves between devices by JAX's collectives and lax.ppermute only.
A program may use at most 128 MiB of HBM per device.

v0:
```python
import jax
import jax.numpy as jnp
from jax import lax
from jax.sharding import Mesh
from jax.sharding import PartitionSpec as P

TP = ("tp_0", "tp_1")
SP_TP = ("sp", "tp_0", "tp_1")
EPSILON = 1e-06
LIMIT = 7.0
SLOPE = 1.702
FLOOR = -1e30


def sent_together(arrays, axis, dim, along):
    both = jnp.concatenate(arrays, axis=along)
    out, at, finished = (lax.all_gather(both, axis, axis=dim, tiled=True), 0, [])
    for a in arrays:
        finished.append(lax.slice_in_dim(out, at, at + a.shape[along], axis=along))
        at += a.shape[along]
    return tuple(finished)


def sum_in_order(tiles, axes, sequence):
    dims = [lax.axis_size(a) for a in axes]
    tiles = tiles.reshape(*dims, *tiles.shape[1:])
    tiles = tiles.transpose(*sequence, *range(len(axes), tiles.ndim))
    tiles = tiles.reshape(-1, *tiles.shape[len(axes) :])
    for k in sequence:
        tiles = lax.psum_scatter(tiles, axes[k], scatter_dimension=0, tiled=True)
    return tiles[0]


def in_blocks(array, dim, length):
    before, after = (array.shape[:dim], array.shape[dim + 1 :])
    return jnp.moveaxis(array.reshape(*before, length, -1, *after), dim, 0)


def sum_by_axis(array, axes, sequence, dim):
    length = lax.axis_size(axes)
    return sum_in_order(in_blocks(array, dim, length), axes, sequence)


def empty_state(heads_here, queries_here, value_width):
    maxima = jnp.full((2, heads_here, queries_here), FLOOR, jnp.float32)
    totals = jnp.zeros((2, heads_here, queries_here), jnp.float32)
    sums = jnp.zeros((2, heads_here, queries_here, value_width), jnp.float32)
    return (maxima, totals, sums)


def absorb_keys(states, queries, keys, values, width):
    maxima, totals, sums = states
    scaling = width ** (-0.5)
    new_maxima = []
    new_totals = []
    new_sums = []
    for which in range(2):
        query_part = queries[:, :, which * width : (which + 1) * width]
        key_part = keys[:, :, which * width : (which + 1) * width]
        scores = (
            jnp.einsum("qhd,khd->hqk", query_part, key_part, preferred_element_type=jnp.float32)
            * scaling
        )
        highest = jnp.maximum(maxima[which], jnp.max(scores, axis=2))
        expo = jnp.exp(scores - highest[:, :, None])
        factor = jnp.exp(maxima[which] - highest)
        new_totals.append(totals[which] * factor + jnp.sum(expo, axis=2))
        carried = jnp.einsum(
            "hqk,khv->hqv", expo.astype(jnp.bfloat16), values, preferred_element_type=jnp.float32
        )
        new_sums.append(sums[which] * factor[:, :, None] + carried)
        new_maxima.append(highest)
    return (jnp.stack(new_maxima), jnp.stack(new_totals), jnp.stack(new_sums))


def finish(states, lambda_row, gain):
    maxima, totals, sums = states
    heard = sums / totals[:, :, :, None]
    differ = heard[0] - lambda_row[:, None, None] * heard[1]
    scaled = lax.rsqrt(jnp.mean(differ * differ, axis=2, keepdims=True) + EPSILON)
    return (differ * scaled * gain).astype(jnp.bfloat16)


def gated_units(grid, w_gate, w_up):
    gate = jnp.einsum("necd,edf->necf", grid, w_gate, preferred_element_type=jnp.float32)
    upward = jnp.einsum("necd,edf->necf", grid, w_up, preferred_element_type=jnp.float32)
    clamped = jnp.minimum(gate, LIMIT)
    return (
        clamped * jax.nn.sigmoid(SLOPE * clamped) * (jnp.clip(upward, -LIMIT, LIMIT) + 1.0)
    ).astype(jnp.bfloat16)


def per_device(
    query_a,
    key_a,
    value_a,
    query_b,
    key_b,
    value_b,
    lambdas,
    gain_a,
    gain_b,
    out_a,
    out_b,
    residual,
    norm_gain,
    route_ids,
    route_weights,
    w_gate,
    w_up,
    w_down,
):
    heads_here = query_a.shape[1]
    queries_here = query_a.shape[0]
    width_a = query_a.shape[2] // 2
    width_b = query_b.shape[2] // 2
    starting = (
        empty_state(heads_here, queries_here, value_a.shape[2]),
        empty_state(heads_here, queries_here, value_b.shape[2]),
    )
    keys_a, values_a, keys_b, values_b = sent_together((key_a, value_a, key_b, value_b), "sp", 0, 2)
    state_a = absorb_keys(starting[0], query_a, keys_a, values_a, width_a)
    state_b = absorb_keys(starting[1], query_b, keys_b, values_b, width_b)
    attended_a = finish(state_a, lambdas[0], gain_a)
    attended_b = finish(state_b, lambdas[1], gain_b)
    model_width = out_a.shape[1]
    weights_a = out_a.reshape(heads_here, -1, model_width)
    weights_b = out_b.reshape(heads_here, -1, model_width)
    first = jnp.einsum("hqv,hvd->qd", attended_a, weights_a, preferred_element_type=jnp.float32)
    projected = lax.psum_scatter(
        (
            first
            + jnp.einsum("hqv,hvd->qd", attended_b, weights_b, preferred_element_type=jnp.float32)
        ).astype(jnp.bfloat16),
        TP,
        scatter_dimension=0,
        tiled=True,
    ).astype(jnp.float32)
    mixed = (residual.astype(jnp.float32) + projected).astype(jnp.bfloat16)
    widened = mixed.astype(jnp.float32)
    normed = (
        widened
        * lax.rsqrt(jnp.mean(widened * widened, axis=1, keepdims=True) + EPSILON)
        * norm_gain
    ).astype(jnp.bfloat16)
    rows_here, chosen = route_ids.shape
    groups = lax.axis_size("sp")
    experts_here = w_gate.shape[0]
    experts_all = experts_here * groups
    capacity = 2 * rows_here * chosen // experts_all
    slots_here = experts_here * capacity
    flat_ids = route_ids.reshape(-1)
    onehot = (flat_ids[:, None] == jnp.arange(experts_all, dtype=jnp.int32)[None, :]).astype(
        jnp.int32
    )
    earlier = jnp.cumsum(onehot, axis=0) - onehot
    target = flat_ids * capacity + jnp.sum(earlier * onehot, axis=1)
    places = jnp.arange(experts_all * capacity, dtype=jnp.int32)
    layout = jnp.any(target.reshape(rows_here, chosen)[None, :, :] == places[:, None, None], axis=2)
    outgoing = jnp.dot(
        layout.astype(jnp.bfloat16), normed, preferred_element_type=jnp.float32
    ).astype(jnp.bfloat16)
    outgoing = outgoing.reshape(groups, slots_here, model_width)
    arrived = lax.all_to_all(outgoing, "sp", split_axis=0, concat_axis=0, tiled=True)
    pieces = lax.all_gather(arrived, TP, axis=0, tiled=True)
    count = pieces.shape[0]
    grid = pieces.reshape(count, experts_here, capacity, model_width)
    active = gated_units(grid, w_gate, w_up)
    down = jnp.einsum("necf,efd->necd", active, w_down, preferred_element_type=jnp.float32)
    partial_value = down.astype(jnp.bfloat16).reshape(count, slots_here, model_width)
    totals = (
        sum_by_axis(partial_value.astype(jnp.float32).astype(jnp.bfloat16), TP, (1, 0), 0)
        .astype(jnp.float32)
        .astype(jnp.bfloat16)
    )
    summed = lax.all_to_all(totals, "sp", split_axis=0, concat_axis=0, tiled=True)
    results = summed.reshape(experts_all * capacity, model_width)
    picked = (
        jnp.take(results, target, axis=0)
        .reshape(rows_here, chosen, model_width)
        .astype(jnp.float32)
    )
    combined = jnp.sum(route_weights[:, :, None] * picked, axis=1)
    return (widened + combined).astype(jnp.bfloat16)


def solution(mesh):
    split = Mesh(mesh.devices.reshape(mesh.shape["sp"], 8, 2), ("sp", "tp_0", "tp_1"))
    placed = (
        P("sp", TP, None),
        P("sp", TP, None),
        P("sp", TP, None),
        P("sp", TP, None),
        P("sp", TP, None),
        P("sp", TP, None),
        P(None, TP),
        P(),
        P(),
        P(TP, None),
        P(TP, None),
        P(SP_TP, None),
        P(),
        P(SP_TP, None),
        P(SP_TP, None),
        P("sp", None, TP),
        P("sp", None, TP),
        P("sp", TP, None),
    )
    return jax.shard_map(
        per_device, mesh=split, in_specs=placed, out_specs=P(SP_TP, None), check_vma=False
    )
```

profile of v0, /device:TPU:1, one launch (start us, length us, event | category | flops | bytes accessed | tf_op | source)
XLA Modules:
  0.0 375.3 jit_solution(6805099216005470352)
XLA Ops:
  6.5 2.0 pad_maximum_fusion
  8.6 1.4 fusion.127
  10.0 69.7 %all-gather.3.cloned.1.call-done = bf16[4096,1,768]{2,0,1:T(8,128)(2,1)} async-done(((bf16[256,1,768]{2,0,1:T(8,128)(2,1)}), bf16[4096,1,768]{2,0,1:T(8,128)(2,1)}) %all-gather.3.cloned.1.call-update) | async-done | bytes 6291472 | tf_op jit(solution)/shard_map/all_gather | solution.py:17
  79.7 2.2 fusion.131
  82.8 0.9 fusion.130
  84.4 1.2 fusion.52
  85.5 1.2 fusion.58
  86.8 0.7 multiply_reduce_fusion.1
  87.5 0.9 fusion.129
  89.0 0.9 fusion.128
  90.6 0.8 fusion.64
  91.4 0.8 fusion.70
  92.3 0.9 multiply_reduce_fusion.2
  93.2 1.5 fusion.101
  94.8 2.9 fusion
  98.6 56.4 %reduce-scatter.4.cloned.1.call-done = bf16[16,4096]{1,0:T(8,128)(2,1)} async-done(((bf16[256,4096]{1,0:T(8,128)(2,1)}), bf16[16,4096]{1,0:T(8,128)(2,1)}) %reduce-scatter.4.cloned.1.call-update) | async-done | bytes 131088 | tf_op jit(solution)/shard_map/reduce_scatter | solution.py:130
  155.0 1.1 fusion.79
  156.1 1.3 convolution_convert_fusion.1
  157.5 15.3 %all_to_all.10 = bf16[16,4,4096]{2,1,0:T(4,128)(2,1)} all-to-all(bf16[16,4,4096]{2,1,0:T(4,128)(2,1)S(1)} %reshape.633), channel_id=1, replica_groups=mesh['sp'=16,'tp_0'=8,'tp_1'=2] {'sp'}, dimensions={0} | all-to-all | bytes 1048576 | tf_op jit(solution)/shard_map/all_to_all | solution.py:164
  172.9 56.6 %all-gather.5.cloned.1.call-done = bf16[256,4,4096]{2,1,0:T(4,128)(2,1)} async-done(((bf16[16,4,4096]{2,1,0:T(4,128)(2,1)}), bf16[256,4,4096]{2,1,0:T(4,128)(2,1)}) %all-gather.5.cloned.1.call-update) | async-done | bytes 8388624 | tf_op jit(solution)/shard_map/all_gather | solution.py:165
  229.6 11.3 %copy.46 = bf16[256,4,4096]{2,0,1:T(8,128)(2,1)} copy(bf16[256,4,4096]{2,1,0:T(4,128)(2,1)} %all-gather.5.cloned.1.call-done) | data formatting | bytes 16777216 | tf_op jit(solution)/shard_map/all_gather | solution.py:165
  240.9 5.7 %fusion.29 = f32[256,2,2,128]{3,0,2,1:T(8,128)S(1)} fusion(bf16[256,2,2,4096]{3,0,2,1:T(8,128)(2,1)} %bitcast.148, bf16[2,4096,128]{2,1,0:T(8,128)(2,1)S(1)} %copy-done.3), kind=kOutput, calls=%fused_computation.36 | convolution fusion | flops 1073872896 | bytes 11010048 | tf_op jit(solution)/shard_map/necd,edf->necf/dot_general | solution.py:85
  246.7 13.4 %convolution_convert_fusion = bf16[2,256,2,4096]{3,1,2,0:T(8,128)(2,1)} fusion(bf16[2,128,4096]{2,1,0:T(8,128)(2,1)S(1)} %copy-done, bf16[256,2,2,4096]{3,0,2,1:T(8,128)(2,1)} %bitcast.149, bf16[2,4096,128]{2,1,0:T(8,128)(2,1)} %param.34, f32[256,2,2,128]{3,0,2,1:T(8,128)S(1)} %fusion.29), kind=kOutput, calls=%fused_computation.1 | convolution fusion | flops 2152857600 | bytes 21495808 | tf_op jit(solution)/shard_map/necf,efd->necd/dot_general | solution.py:169
  260.1 7.7 %copy.47 = bf16[8,2,16,4,4096]{4,2,3,0,1:T(8,128)(2,1)} copy(bf16[8,2,16,4,4096]{4,2,1,0,3:T(8,128)(2,1)} %bitcast.151) | data formatting | bytes 16777216 | tf_op jit(solution)/shard_map/reshape;reshape | solution.py:26
  267.9 20.6 %reduce-scatter.6.cloned.1.call-done = bf16[8,16,4,4096]{3,1,2,0:T(8,128)(2,1)} async-done(((bf16[16,16,4,4096]{3,1,2,0:T(8,128)(2,1)}), bf16[8,16,4,4096]{3,1,2,0:T(8,128)(2,1)}) %reduce-scatter.6.cloned.1.call-update) | async-done | bytes 4194320 | tf_op jit(solution)/shard_map/reduce_scatter | solution.py:30
  288.5 58.4 %reduce-scatter.8.cloned.1.call-done = bf16[1,16,4,4096]{3,1,2,0:T(8,128)(2,1)} async-done(((bf16[8,16,4,4096]{3,1,2,0:T(8,128)(2,1)}), bf16[1,16,4,4096]{3,1,2,0:T(8,128)(2,1)}) %reduce-scatter.8.cloned.1.call-update) | async-done | bytes 524304 | tf_op jit(solution)/shard_map/reduce_scatter | solution.py:30
  346.9 2.2 copy.48
  349.2 6.5 %all-to-all-start.1 = ((bf16[16,4,4096]{2,1,0:T(4,128)(2,1)}), bf16[16,4,4096]{2,1,0:T(4,128)(2,1)S(1)}, u32[]{:S(2)}, u32[]{:S(2)}) async-start(bf16[16,4,4096]{2,1,0:T(4,128)(2,1)} %copy.48), calls=%async_computation.4 | async-start | bytes 1048576 | tf_op jit(solution)/shard_map/all_to_all | solution.py:176
  356.1 10.1 %all-to-all-done.1 = bf16[16,4,4096]{2,1,0:T(4,128)(2,1)S(1)} async-done(((bf16[16,4,4096]{2,1,0:T(4,128)(2,1)}), bf16[16,4,4096]{2,1,0:T(4,128)(2,1)S(1)}, u32[]{:S(2)}, u32[]{:S(2)}) %all-to-all-start.1) | async-done | bytes 524320 | tf_op jit(solution)/shard_map/all_to_all | solution.py:176
  366.3 0.7 gather_fusion
  367.2 0.8 multiply_reduce_fusion
  368.1 0.7 fusion.82
  (76 shorter events, 5.0 us)
Async XLA Ops:
  6.5 240.1 %copy-start = (bf16[2,128,4096]{2,1,0:T(8,128)(2,1)S(1)}, bf16[2,128,4096]{2,1,0:T(8,128)(2,1)}, u32[]{:S(2)}) copy-start(bf16[2,128,4096]{2,1,0:T(8,128)(2,1)} %param.35) | copy-start | bytes 6291460
  6.5 73.2 %all-gather.3.cloned.1.call-start = ((), (), s32[]{:S(2)}) async-start(), calls=%async_computation.5 | async-start | bytes 6684672 | tf_op jit(solution)/shard_map/all_gather | solution.py:17
  8.5 146.5 %reduce-scatter.4.cloned.1.call-start = ((), (), s32[]{:S(2)}) async-start(), calls=%async_computation.6 | async-start | bytes 2228224 | tf_op jit(solution)/shard_map/reduce_scatter | solution.py:130
  10.0 72.6 %copy-start.8 = (bf16[256,1,256]{2,0,1:T(8,128)(2,1)S(1)}, bf16[256,1,256]{2,0,1:T(8,128)(2,1)}, u32[]{:S(2)}) copy-start(bf16[256,1,256]{2,0,1:T(8,128)(2,1)} %param.18) | copy-start | bytes 393220
  79.7 3.1 copy-start.1
  85.5 1.9 copy-start.7
  91.4 1.8 copy-start.6
  91.4 1.8 copy-start.11
  92.3 2.4 copy-start.2
  92.3 2.4 copy-start.12
  94.7 3.2 copy-start.10
  94.7 60.3 %copy-start.4 = (bf16[16,4096]{1,0:T(8,128)(2,1)S(1)}, bf16[16,4096]{1,0:T(8,128)(2,1)}, u32[]{:S(2)}) copy-start(bf16[16,4096]{1,0:T(8,128)(2,1)} %param.29) | copy-start | bytes 393220
  94.8 61.3 %copy-start.9 = (f32[4096]{0:T(1024)S(1)}, f32[4096]{0:T(1024)}, u32[]{:S(2)}) copy-start(f32[4096]{0:T(1024)} %param.30) | copy-start | bytes 49156
  97.6 131.9 %all-gather.5.cloned.1.call-start = ((), (), s32[]{:S(2)}) async-start(), calls=%async_computation.7 | async-start | bytes 8912896 | tf_op jit(solution)/shard_map/all_gather | solution.py:165
  172.9 115.6 %reduce-scatter.6.cloned.1.call-start = ((), (), s32[]{:S(2)}) async-start(), calls=%async_computation.8 | async-start | bytes 12582912 | tf_op jit(solution)/shard_map/reduce_scatter | solution.py:30
  229.6 11.3 %copy-start.3 = (bf16[2,4096,128]{2,1,0:T(8,128)(2,1)S(1)}, bf16[2,4096,128]{2,1,0:T(8,128)(2,1)}, u32[]{:S(2)}) copy-start(bf16[2,4096,128]{2,1,0:T(8,128)(2,1)} %param.33) | copy-start | bytes 6291460
  267.8 88.2 %copy-start.13 = (f32[16,2]{0,1:T(2,128)S(1)}, f32[16,2]{0,1:T(2,128)}, u32[]{:S(2)}) copy-start(f32[16,2]{0,1:T(2,128)} %param.32) | copy-start | bytes 388
  267.8 79.1 %reduce-scatter.8.cloned.1.call-start = ((), (), s32[]{:S(2)}) async-start(), calls=%async_computation.9 | async-start | bytes 4718592 | tf_op jit(solution)/shard_map/reduce_scatter | solution.py:30
  288.5 79.5 %copy-start.5 = (bf16[16,4096]{1,0:T(8,128)(2,1)S(1)}, bf16[16,4096]{1,0:T(8,128)(2,1)}, u32[]{:S(2)}) copy-start(bf16[16,4096]{1,0:T(8,128)(2,1)} %reduce-scatter.4.cloned.1.call-done) | copy-start | bytes 393220
  349.2 17.0 %all-to-all-start.1 = ((bf16[16,4,4096]{2,1,0:T(4,128)(2,1)}), bf16[16,4,4096]{2,1,0:T(4,128)(2,1)S(1)}, u32[]{:S(2)}, u32[]{:S(2)}) async-start(bf16[16,4,4096]{2,1,0:T(4,128)(2,1)} %copy.48), calls=%async_computation.4 | async-start | bytes 1048576 | tf_op jit(solution)/shard_map/all_to_all | solution.py:176
Sparse Core Ops, SparseCore 0:
  9.8 69.8 all-gather.2
  97.8 57.1 reduce-scatter.3
  173.0 56.5 all-gather.4
  267.9 20.5 reduce-scatter.5
  290.9 55.9 reduce-scatter.7
where the time goes:
time: 376 us; the launch traced here: 375 us
  waiting for transfers between devices  272 us (72%)
  matrix products  33.6 us (9%)
  local copies, waits for them, and re-layouts  24.9 us (7%)
  blocking collectives  15.3 us (4%)
  between operations  13.5 us (4%)
  other arithmetic  9.25 us (2%)
  starting transfers between devices  6.87 us (2%)
    reduce_scatter x2, waiting for transfers between devices, sum_in_order(): tiles = lax.psum_scatter(tiles, axes[k], scatter_dimension=0, tiled=True)  79 us
    all_gather x1, waiting for transfers between devices, sent_together(): lax.all_gather(both, axis, axis=dim, tiled=True)  69.7 us
    all_gather x1, waiting for transfers between devices, per_device(): pieces = lax.all_gather(arrived, TP, axis=0, tiled=True)  56.6 us
    reduce_scatter x1, waiting for transfers between devices, per_device(): lax.psum_scatter((first + jnp.einsum('hqv,hvd->qd', attended_b, weights_b...  56.4 us
    all_to_all x1, blocking collectives, per_device(): lax.all_to_all(outgoing, 'sp', split_axis=0, concat_axis=0, tiled=True)  15.3 us
    dot_general x1, matrix products, per_device(): jnp.einsum('necf,efd->necd', active, w_down, preferred_element_type=jnp.f...  13.4 us
    all_gather x1, local copies, waits for them, and re-layouts, per_device(): pieces = lax.all_gather(arrived, TP, axis=0, tiled=True)  11.3 us
    all_to_all x1, waiting for transfers between devices, per_device(): lax.all_to_all(totals, 'sp', split_axis=0, concat_axis=0, tiled=True)  10.1 us
  transfers between devices with their start and end apart: 6, of which 6 were waited for; matrix products, arithmetic and copies ran while one was open for 1% of the time, Pallas kernels for 0%

commit v1 on v0

--- a/solution.py
+++ b/solution.py
@@ -162,7 +162,8 @@
     ).astype(jnp.bfloat16)
     outgoing = outgoing.reshape(groups, slots_here, model_width)
     arrived = lax.all_to_all(outgoing, "sp", split_axis=0, concat_axis=0, tiled=True)
-    pieces = lax.all_gather(arrived, TP, axis=0, tiled=True)
+    stack = jnp.stack([arrived] * lax.axis_size(TP))
+    pieces = jnp.concatenate(lax.all_to_all(stack, TP, 0, 0), axis=0)
     count = pieces.shape[0]
     grid = pieces.reshape(count, experts_here, capacity, model_width)
     active = gated_units(grid, w_gate, w_up)

time: 376 us -> 508 us (1.35)
  blocking collectives: 15.3 us -> 211 us
  waiting for transfers between devices: 272 us -> 210 us
    all_to_all x0 -> x1, blocking collectives: none -> 196 us  [per_device(): pieces = jnp.concatenate(lax.all_to_all(stack, TP, 0, 0), axis=0)]
    all_gather x1 -> x0, waiting for transfers between devices: 56.6 us -> none  [per_device(): pieces = lax.all_gather(arrived, TP, axis=0, tiled=True)]
    all_gather x1 -> x0, local copies, waits for them, and re-layouts: 11.3 us -> none  [per_device(): pieces = lax.all_gather(arrived, TP, axis=0, tiled=True)]
    all_to_all x0 -> x2, local copies, waits for them, and re-layouts: none -> 8.15 us  [the longest x1 7.86 us: per_device(): pieces = jnp.concatenate(lax.all_to_all(stack, TP, 0, 0), axis=0)]
    reduce_scatter x2, waiting for transfers between devices: 79 us -> 73.8 us  [sum_in_order(): tiles = lax.psum_scatter(tiles, axes[k], scatter_dimension=0, tiled=True)]
  transfers between devices with their start and end apart: 6 -> 5, of which waited for: 6 -> 5; matrix products, arithmetic and copies ran while one was open for 1% -> 0% of each run, Pallas kernels for 0% -> 0%
where the time goes in v1:
time: 508 us; the launch traced here: 507 us
  blocking collectives  211 us (42%)
  waiting for transfers between devices  210 us (41%)
  matrix products  33.6 us (7%)
  local copies, waits for them, and re-layouts  22.8 us (4%)
  between operations  13.5 us (3%)
  other arithmetic  9.25 us (2%)
  starting transfers between devices  6.85 us (1%)
    all_to_all x1, blocking collectives, per_device(): pieces = jnp.concatenate(lax.all_to_all(stack, TP, 0, 0), axis=0)  196 us
    reduce_scatter x2, waiting for transfers between devices, sum_in_order(): tiles = lax.psum_scatter(tiles, axes[k], scatter_dimension=0, tiled=True)  73.8 us
    all_gather x1, waiting for transfers between devices, sent_together(): lax.all_gather(both, axis, axis=dim, tiled=True)  69.7 us
    reduce_scatter x1, waiting for transfers between devices, per_device(): lax.psum_scatter((first + jnp.einsum('hqv,hvd->qd', attended_b, weights_b...  56.4 us
    all_to_all x1, blocking collectives, per_device(): lax.all_to_all(outgoing, 'sp', split_axis=0, concat_axis=0, tiled=True)  15.2 us
    dot_general x1, matrix products, per_device(): jnp.einsum('necf,efd->necd', active, w_down, preferred_element_type=jnp.f...  13.4 us
  transfers between devices with their start and end apart: 5, of which 5 were waited for; matrix products, arithmetic and copies ran while one was open for 0% of the time, Pallas kernels for 0%

profile of v1, /device:TPU:1, one launch (start us, length us, event | category | flops | bytes accessed | tf_op | source)
XLA Modules:
  0.0 507.2 jit_solution(2465910042576922622)
XLA Ops:
  6.5 2.0 pad_maximum_fusion
  8.6 1.4 fusion.127
  10.0 69.7 %all-gather.2.cloned.1.call-done = bf16[4096,1,768]{2,0,1:T(8,128)(2,1)} async-done(((bf16[256,1,768]{2,0,1:T(8,128)(2,1)}), bf16[4096,1,768]{2,0,1:T(8,128)(2,1)}) %all-gather.2.cloned.1.call-update) | async-done | bytes 6291472 | tf_op jit(solution)/shard_map/all_gather | solution.py:17
  79.7 2.2 fusion.131
  82.8 0.9 fusion.130
  84.4 1.2 fusion.52
  85.5 1.2 fusion.58
  86.8 0.7 multiply_reduce_fusion.1
  87.5 0.9 fusion.129
  89.0 0.9 fusion.128
  90.6 0.8 fusion.64
  91.4 0.8 fusion.70
  92.3 0.9 multiply_reduce_fusion.2
  93.2 1.5 fusion.101
  94.8 2.9 fusion
  98.6 56.4 %reduce-scatter.4.cloned.1.call-done = bf16[16,4096]{1,0:T(8,128)(2,1)} async-done(((bf16[256,4096]{1,0:T(8,128)(2,1)}), bf16[16,4096]{1,0:T(8,128)(2,1)}) %reduce-scatter.4.cloned.1.call-update) | async-done | bytes 131088 | tf_op jit(solution)/shard_map/reduce_scatter | solution.py:130
  155.0 1.1 fusion.79
  156.1 1.3 convolution_convert_fusion.1
  157.5 15.2 %all_to_all.15 = bf16[16,4,4096]{2,1,0:T(4,128)(2,1)S(1)} all-to-all(bf16[16,4,4096]{2,1,0:T(4,128)(2,1)S(1)} %reshape.632), channel_id=1, replica_groups=mesh['sp'=16,'tp_0'=8,'tp_1'=2] {'sp'}, dimensions={0} | all-to-all | bytes 1048576 | tf_op jit(solution)/shard_map/all_to_all | solution.py:164
  173.1 1.1 stack.26
  174.1 196.0 %all_to_all.16 = bf16[16,16,4,4096]{3,1,2,0:T(8,128)(2,1)} all-to-all(bf16[16,16,4,4096]{3,1,2,0:T(8,128)(2,1)S(1)} %stack.26), channel_id=1, replica_groups=mesh['sp'=16,'tp_0'=8,'tp_1'=2] {'tp_0','tp_1'}, dimensions={0} | all-to-all | bytes 16777216 | tf_op jit(solution)/shard_map/all_to_all | solution.py:166
  370.1 7.9 %copy.49 = bf16[16,16,4,4096]{3,1,0,2:T(8,128)(2,1)} copy(bf16[16,16,4,4096]{3,1,2,0:T(8,128)(2,1)} %all_to_all.16) | data formatting | bytes 16777216 | tf_op jit(solution)/shard_map/all_to_all | solution.py:166
  378.0 5.7 %fusion.29 = f32[256,2,2,128]{3,0,2,1:T(8,128)S(1)} fusion(bf16[256,2,2,4096]{3,0,2,1:T(8,128)(2,1)} %bitcast.148, bf16[2,4096,128]{2,1,0:T(8,128)(2,1)S(1)} %copy-done.3), kind=kOutput, calls=%fused_computation.36 | convolution fusion | flops 1073872896 | bytes 11010048 | tf_op jit(solution)/shard_map/necd,edf->necf/dot_general | solution.py:85
  383.7 13.4 %convolution_convert_fusion = bf16[2,256,2,4096]{3,1,2,0:T(8,128)(2,1)} fusion(bf16[2,128,4096]{2,1,0:T(8,128)(2,1)S(1)} %copy-done, bf16[256,2,2,4096]{3,0,2,1:T(8,128)(2,1)} %bitcast.149, bf16[2,4096,128]{2,1,0:T(8,128)(2,1)} %param.34, f32[256,2,2,128]{3,0,2,1:T(8,128)S(1)} %fusion.29), kind=kOutput, calls=%fused_computation.1 | convolution fusion | flops 2152857600 | bytes 21495808 | tf_op jit(solution)/shard_map/necf,efd->necd/dot_general | solution.py:170
  397.1 7.7 %copy.50 = bf16[8,2,16,4,4096]{4,2,3,0,1:T(8,128)(2,1)} copy(bf16[8,2,16,4,4096]{4,2,1,0,3:T(8,128)(2,1)} %bitcast.151) | data formatting | bytes 16777216 | tf_op jit(solution)/shard_map/reshape;reshape | solution.py:26
  404.9 15.4 %reduce-scatter.6.cloned.1.call-done = bf16[8,16,4,4096]{3,1,2,0:T(8,128)(2,1)} async-done(((bf16[16,16,4,4096]{3,1,2,0:T(8,128)(2,1)}), bf16[8,16,4,4096]{3,1,2,0:T(8,128)(2,1)}) %reduce-scatter.6.cloned.1.call-update) | async-done | bytes 4194320 | tf_op jit(solution)/shard_map/reduce_scatter | solution.py:30
  420.4 58.4 %reduce-scatter.8.cloned.1.call-done = bf16[1,16,4,4096]{3,1,2,0:T(8,128)(2,1)} async-done(((bf16[8,16,4,4096]{3,1,2,0:T(8,128)(2,1)}), bf16[1,16,4,4096]{3,1,2,0:T(8,128)(2,1)}) %reduce-scatter.8.cloned.1.call-update) | async-done | bytes 524304 | tf_op jit(solution)/shard_map/reduce_scatter | solution.py:30
  478.8 2.3 copy.51
  481.0 6.5 %all-to-all-start.2 = ((bf16[16,4,4096]{2,1,0:T(4,128)(2,1)}), bf16[16,4,4096]{2,1,0:T(4,128)(2,1)S(1)}, u32[]{:S(2)}, u32[]{:S(2)}) async-start(bf16[16,4,4096]{2,1,0:T(4,128)(2,1)} %copy.51), calls=%async_computation.5 | async-start | bytes 1048576 | tf_op jit(solution)/shard_map/all_to_all | solution.py:177
  488.0 10.1 %all-to-all-done.2 = bf16[16,4,4096]{2,1,0:T(4,128)(2,1)S(1)} async-done(((bf16[16,4,4096]{2,1,0:T(4,128)(2,1)}), bf16[16,4,4096]{2,1,0:T(4,128)(2,1)S(1)}, u32[]{:S(2)}, u32[]{:S(2)}) %all-to-all-start.2) | async-done | bytes 524320 | tf_op jit(solution)/shard_map/all_to_all | solution.py:177
  498.2 0.7 gather_fusion
  499.1 0.8 multiply_reduce_fusion
  (76 shorter events, 6.0 us)
Async XLA Ops:
  6.5 377.2 %copy-start = (bf16[2,128,4096]{2,1,0:T(8,128)(2,1)S(1)}, bf16[2,128,4096]{2,1,0:T(8,128)(2,1)}, u32[]{:S(2)}) copy-start(bf16[2,128,4096]{2,1,0:T(8,128)(2,1)} %param.35) | copy-start | bytes 6291460
  6.5 73.2 %all-gather.2.cloned.1.call-start = ((), (), s32[]{:S(2)}) async-start(), calls=%async_computation.6 | async-start | bytes 6684672 | tf_op jit(solution)/shard_map/all_gather | solution.py:17
  8.5 146.5 %reduce-scatter.4.cloned.1.call-start = ((), (), s32[]{:S(2)}) async-start(), calls=%async_computation.7 | async-start | bytes 2228224 | tf_op jit(solution)/shard_map/reduce_scatter | solution.py:130
  10.0 72.6 %copy-start.8 = (bf16[256,1,256]{2,0,1:T(8,128)(2,1)S(1)}, bf16[256,1,256]{2,0,1:T(8,128)(2,1)}, u32[]{:S(2)}) copy-start(bf16[256,1,256]{2,0,1:T(8,128)(2,1)} %param.18) | copy-start | bytes 393220
  79.7 3.1 copy-start.1
  85.5 1.9 copy-start.7
  91.4 1.8 copy-start.6
  91.4 1.8 copy-start.11
  92.3 2.4 copy-start.2
  92.3 2.4 copy-start.12
  94.7 3.2 copy-start.10
  94.7 60.3 %copy-start.4 = (bf16[16,4096]{1,0:T(8,128)(2,1)S(1)}, bf16[16,4096]{1,0:T(8,128)(2,1)}, u32[]{:S(2)}) copy-start(bf16[16,4096]{1,0:T(8,128)(2,1)} %param.29) | copy-start | bytes 393220
  94.8 61.3 %copy-start.9 = (f32[4096]{0:T(1024)S(1)}, f32[4096]{0:T(1024)}, u32[]{:S(2)}) copy-start(f32[4096]{0:T(1024)} %param.30) | copy-start | bytes 49156
  97.6 322.7 %reduce-scatter.6.cloned.1.call-start = ((), (), s32[]{:S(2)}) async-start(), calls=%async_computation.8 | async-start | bytes 12582912 | tf_op jit(solution)/shard_map/reduce_scatter | solution.py:30
  370.1 7.9 %copy-start.3 = (bf16[2,4096,128]{2,1,0:T(8,128)(2,1)S(1)}, bf16[2,4096,128]{2,1,0:T(8,128)(2,1)}, u32[]{:S(2)}) copy-start(bf16[2,4096,128]{2,1,0:T(8,128)(2,1)} %param.33) | copy-start | bytes 6291460
  404.9 83.0 %copy-start.13 = (f32[16,2]{0,1:T(2,128)S(1)}, f32[16,2]{0,1:T(2,128)}, u32[]{:S(2)}) copy-start(f32[16,2]{0,1:T(2,128)} %param.32) | copy-start | bytes 388
  404.9 73.9 %reduce-scatter.8.cloned.1.call-start = ((), (), s32[]{:S(2)}) async-start(), calls=%async_computation.9 | async-start | bytes 4718592 | tf_op jit(solution)/shard_map/reduce_scatter | solution.py:30
  420.4 79.5 %copy-start.5 = (bf16[16,4096]{1,0:T(8,128)(2,1)S(1)}, bf16[16,4096]{1,0:T(8,128)(2,1)}, u32[]{:S(2)}) copy-start(bf16[16,4096]{1,0:T(8,128)(2,1)} %reduce-scatter.4.cloned.1.call-done) | copy-start | bytes 393220
  481.0 17.0 %all-to-all-start.2 = ((bf16[16,4,4096]{2,1,0:T(4,128)(2,1)}), bf16[16,4,4096]{2,1,0:T(4,128)(2,1)S(1)}, u32[]{:S(2)}, u32[]{:S(2)}) async-start(bf16[16,4,4096]{2,1,0:T(4,128)(2,1)} %copy.51), calls=%async_computation.5 | async-start | bytes 1048576 | tf_op jit(solution)/shard_map/all_to_all | solution.py:177
Sparse Core Ops, SparseCore 0:
  9.8 69.8 all-gather.1
  97.8 57.1 reduce-scatter.3
  405.0 15.3 reduce-scatter.5
  422.8 55.9 reduce-scatter.7
